TPU v7x, 32 devices: a whole 2x2x4 slice. The times are simulated.
32 devices in a mesh: fs: 16 (over z, y, x), tp: 2 (over core).
Axes of the slice: x: 2, y: 2, z: 4, core: 2. Of those that a mesh axis runs over, the one named last changes fastest.
Arguments:
- saved_inputs: bfloat16 [2048, 4096], P('fs', 'tp'), may hold values from -6 to 6
- value_cotangent: bfloat16 [2048, 2048], P('fs'), may hold values from -0.1875 to 0.1875
- glu_output: bfloat16 [2048, 2048], P('fs', 'tp'), may hold values from -6 to 6
- conv_cotangent: bfloat16 [2048, 2048], P('fs', 'tp'), may hold values from -0.125 to 0.125
- factor: bfloat16 [4096, 256], P('tp'), may hold values from -0.09375 to 0.09375
- value_weight: float32 [2048, 4096], P('fs', 'tp'), may hold values from -3 to 3
- first_moment: float32 [2048, 256], P('fs', 'tp'), may hold values from -6 to 6
- second_moment: float32 [2048, 256], P('fs', 'tp'), may hold values from 0.25 to 4
- kernel: float32 [31, 2048], P(None, 'tp'), may hold values from -1 to 1
- kernel_first: float32 [31, 2048], P(None, 'tp'), may hold values from -6 to 6
- kernel_second: float32 [31, 2048], P(None, 'tp'), may hold values from 0.25 to 4
Outputs:
- new_value: float32 [2048, 4096], P('fs', 'tp')
- value_copy: bfloat16 [2048, 4096], P('fs', 'tp')
- value_step: float32 [2048, 4096], P('fs', 'tp')
- new_first: float32 [2048, 256], P('fs', 'tp')
- new_second: float32 [2048, 256], P('fs', 'tp')
- new_kernel: float32 [31, 2048], P(None, 'tp')
- new_kernel_first: float32 [31, 2048], P(None, 'tp')
- new_kernel_second: float32 [31, 2048], P(None, 'tp')
All inputs are finite; a program needn't handle non-finite values.
Results may differ from a plain program's by a relative error of at most 0.0055.
Values may be sent and summed in bfloat16 or wider, within the bound.
A program may use at most 64 MiB of HBM per device.

v0:
```python
import functools

import jax
import jax.numpy as jnp
from jax import lax
from jax.experimental import pallas as pl
from jax.experimental.pallas import tpu as pltpu
from jax.sharding import PartitionSpec as P

MESH = pl.DeviceIdType.MESH
LANES = 128
f32 = jnp.float32
bf16 = jnp.bfloat16


def remote(src, dst, send, recv, axis, peer):
    return pltpu.make_async_remote_copy(
        src_ref=src,
        dst_ref=dst,
        send_sem=send,
        recv_sem=recv,
        device_id={axis: peer},
        device_id_type=MESH,
    )


def reduce_kernel(
    n,
    m,
    x_hbm,
    v_hbm,
    g_hbm,
    c_hbm,
    f_hbm,
    m1_hbm,
    m2_hbm,
    proj_ref,
    kg_ref,
    dn_ref,
    x_ref,
    v_ref,
    g_ref,
    c_ref,
    f_ref,
    m1_ref,
    m2_ref,
    load_s,
    low_out,
    low_in,
    gram,
    part,
    recv,
    halo,
    ext,
    cot,
    stage,
    tap_out,
    tap_in,
    tap_all,
    dirs,
    low_s,
    low_r,
    gram_s,
    gram_r,
    bulk_s,
    bulk_r,
    halo_s,
    halo_r,
    tap_s,
    tap_r,
    all_s,
    all_r,
    dir_s,
    dir_r,
):
    me = lax.axis_index("fs")
    my = lax.axis_index("tp")
    tokens = x_ref.shape[0]
    width = f_ref.shape[0] * m
    rows, cols = m1_ref.shape
    reach = halo.shape[0]
    groups = ext.shape[0]
    taps = kg_ref.shape[0]
    padded = stage.shape[0] // groups

    def peers(count, own, fn):
        def step(off, carry):
            fn(off, lax.rem(own + off, count))
            return carry

        lax.fori_loop(1, count, step, 0)

    def far_first(fn):
        half = n // 2
        side, place = me // half, lax.rem(me, half)

        def across(j, carry):
            fn(j, (1 - side) * half + lax.rem(place + j, half))
            return carry

        def along(j, carry):
            fn(half + j, side * half + lax.rem(place + j, half))
            return carry

        lax.fori_loop(0, half, across, 0)
        lax.fori_loop(1, half, along, 0)

    barrier = pltpu.get_barrier_semaphore()
    peers(n, me, lambda off, p: pl.semaphore_signal(barrier, inc=1, device_id={"fs": p}, device_id_type=MESH))
    peers(m, my, lambda off, p: pl.semaphore_signal(barrier, inc=1, device_id={"tp": p}, device_id_type=MESH))

    pairs = [(x_hbm, x_ref), (f_hbm, f_ref), (g_hbm, g_ref), (c_hbm, c_ref)]
    pairs += [(v_hbm, v_ref), (m1_hbm, m1_ref), (m2_hbm, m2_ref)]
    loads = [pltpu.make_async_copy(a, b, load_s.at[i]) for i, (a, b) in enumerate(pairs)]
    for load in loads:
        load.start()
    loads[0].wait()
    loads[1].wait()

    low = jnp.dot(x_ref[...], f_ref[...], preferred_element_type=f32).astype(bf16)
    for j in range(m):
        low_out[j] = low[:, j * cols : (j + 1) * cols]

    loads[2].wait()
    loads[3].wait()
    for g in range(groups):
        lanes = slice(g * LANES, (g + 1) * LANES)
        ext[g, :reach] = jnp.zeros((reach, LANES), f32)
        ext[g, reach:] = g_ref[:, lanes].astype(f32)
        cot[g] = c_ref[:, lanes].astype(f32)

    def group_step(count, add):
        def step(g, carry):
            right = cot[g, :count, :]
            sums = []
            for k in range(taps):
                product = ext[g, pl.ds(reach - k, count), :] * right
                sums.append(jnp.sum(product, axis=0, keepdims=True))
            sums.append(jnp.zeros((padded - taps, LANES), f32))
            at = pl.ds(pl.multiple_of(g * padded, padded), padded)
            block = jnp.concatenate(sums, axis=0)
            stage[at, :] = stage[at, :] + block if add else block
            return carry

        lax.fori_loop(0, groups, step, 0)

    group_step(tokens, False)

    pl.semaphore_wait(barrier, n - 1 + m - 1)

    def low_copy(off, p):
        return remote(low_out.at[p], low_in.at[my], low_s.at[off], low_r.at[off], "tp", p)

    peers(m, my, lambda off, p: low_copy(off, p).start())
    low_in[my] = low_out[my]
    after = lax.rem(me + 1, n)
    halo_copy = remote(
        g_ref.at[pl.ds(tokens - reach, reach)], halo, halo_s, halo_r, "fs", after
    )
    halo_copy.start()

    halo_copy.wait()
    halo_f = jnp.where(me > 0, halo[...].astype(f32), 0.0)
    for g in range(groups):
        ext[g, :reach] = halo_f[:, g * LANES : (g + 1) * LANES]
        ext[g, reach:] = jnp.zeros((tokens, LANES), f32)
    group_step(reach, True)
    tap_out[...] = stage[...].reshape(tap_out.shape).astype(bf16)

    def tap_copy(off, p):
        return remote(tap_out.at[p], tap_in.at[me], tap_s.at[off], tap_r.at[off], "fs", p)

    peers(n, me, lambda off, p: tap_copy(off, p).start())
    tap_in[me] = tap_out[me]
    loads[4].wait()

    peers(m, my, lambda off, p: low_copy(off, p).wait())
    reduced = low_in[0].astype(f32)
    for j in range(1, m):
        reduced = reduced + low_in[j].astype(f32)
    reduced = reduced.astype(bf16)

    part[...] = (
        lax.dot_general(v_ref[...], reduced, (((0,), (0,)), ((), ())), preferred_element_type=f32)
        .astype(bf16)
        .reshape(n, rows, cols)
    )

    def bulk_copy(off, p):
        return remote(part.at[p], recv.at[me], bulk_s.at[off], bulk_r.at[off], "fs", p)

    far_first(lambda off, p: bulk_copy(off, p).start())
    recv[me] = part[me]

    gram[my] = lax.dot_general(
        f_ref[...], f_ref[...], (((0,), (0,)), ((), ())), preferred_element_type=f32
    )

    def gram_copy(off, p):
        return remote(gram.at[my], gram.at[my], gram_s.at[off], gram_r.at[off], "tp", p)

    peers(m, my, lambda off, p: gram_copy(off, p).start())

    peers(n, me, lambda off, p: tap_copy(off, p).wait())
    tap_all[me] = jnp.sum(tap_in[...].astype(f32), axis=0).astype(bf16)

    def all_copy(off, p):
        return remote(tap_all.at[me], tap_all.at[me], all_s.at[off], all_r.at[off], "fs", p)

    peers(n, me, lambda off, p: all_copy(off, p).start())

    loads[5].wait()
    loads[6].wait()
    far_first(lambda off, p: bulk_copy(off, p).wait())
    projected = recv[0].astype(f32)
    for j in range(1, n):
        projected = projected + recv[j].astype(f32)
    proj_ref[...] = projected
    first = 0.8 * m1_ref[...] + 0.2 * projected
    second = 0.9 * m2_ref[...] + 0.1 * projected * projected
    dirs[my] = first / jnp.sqrt(second)

    def dir_copy(off, p):
        return remote(dirs.at[my], dirs.at[my], dir_s.at[off], dir_r.at[off], "tp", p)

    peers(m, my, lambda off, p: dir_copy(off, p).start())

    peers(m, my, lambda off, p: gram_copy(off, p).wait())
    total = gram[0]
    for j in range(1, m):
        total = total + gram[j]
    peers(m, my, lambda off, p: dir_copy(off, p).wait())
    direction = jnp.concatenate([dirs[j] for j in range(m)], axis=1)
    turned = jnp.dot(direction, total, precision=lax.Precision.HIGHEST, preferred_element_type=f32)
    mean = jnp.sum(turned * direction, axis=1, keepdims=True) / width
    dn_ref[...] = (direction / jnp.sqrt(mean + 0.01)).astype(bf16)

    peers(n, me, lambda off, p: all_copy(off, p).wait())
    stage[...] = tap_all[...].astype(f32).reshape(stage.shape)
    for g in range(groups):
        kg_ref[:, g * LANES : (g + 1) * LANES] = stage[g * padded : g * padded + taps, :]


def update_kernel(steps, *refs):
    source, target, local, made = refs[:10], refs[10:18], refs[18:28], refs[28:36]
    small_s, f_s, w_s, out_s, wide_s = refs[36:]
    dn_ref, f_ref, w_ref, proj_ref, m1_ref, m2_ref, kg_ref, k_ref, k1_ref, k2_ref = local
    value_ref, copy_ref, step_ref, n1_ref, n2_ref, nk_ref, nk1_ref, nk2_ref = made
    block = f_ref.shape[0] // steps
    spans = [pl.ds(i * block, block) for i in range(steps)]
    copy = pltpu.make_async_copy
    small = {i: copy(source[i], local[i], small_s.at[i]) for i in (0, 3, 4, 5, 6, 7, 8, 9)}
    f_in = [copy(source[1].at[at], f_ref.at[at], f_s.at[i]) for i, at in enumerate(spans)]
    w_in = [copy(source[2].at[:, at], w_ref.at[:, at], w_s.at[i]) for i, at in enumerate(spans)]
    small[0].start()
    for i in range(steps):
        f_in[i].start()
        w_in[i].start()
    for i in range(3, 10):
        small[i].start()

    outs = []
    dims = (((1,), (1,)), ((), ()))
    small[0].wait()
    dn = dn_ref[...]
    for i, at in enumerate(spans):
        f_in[i].wait()
        step = lax.dot_general(dn, f_ref[at, :], dims, preferred_element_type=f32)
        w_in[i].wait()
        step_ref[:, at] = step
        value = w_ref[:, at] - 0.05 * step
        value_ref[:, at] = value
        copy_ref[:, at] = value.astype(bf16)
        for j in range(3):
            out = copy(made[j].at[:, at], target[j].at[:, at], wide_s.at[j, i])
            out.start()
            outs.append(out)

    for i in range(3, 10):
        small[i].wait()
    projected = proj_ref[...]
    n1_ref[...] = 0.8 * m1_ref[...] + 0.2 * projected
    n2_ref[...] = 0.9 * m2_ref[...] + 0.1 * projected * projected
    grad = kg_ref[...]
    first = 0.8 * k1_ref[...] + 0.2 * grad
    second = 0.9 * k2_ref[...] + 0.1 * grad * grad
    nk1_ref[...] = first
    nk2_ref[...] = second
    nk_ref[...] = k_ref[...] - 0.05 * first / jnp.sqrt(second)
    for j in range(3, 8):
        out = copy(made[j], target[j], out_s.at[j])
        out.start()
        outs.append(out)
    for out in outs:
        out.wait()


def body(n, m, x, v, g, c, f, w, m1, m2, k, k1, k2):
    tokens = x.shape[0]
    features, rank = f.shape
    rows, cols = m1.shape
    taps, channels = k.shape
    groups = channels // LANES
    reach = -(-(taps - 1) // 16) * 16
    padded = -(-taps // 8) * 8
    chunk = groups * padded // n
    vmem = pl.BlockSpec(memory_space=pltpu.VMEM)
    dma = pltpu.SemaphoreType.DMA
    proj, kg, dn = pl.pallas_call(
        functools.partial(reduce_kernel, n, m),
        out_shape=(
            jax.ShapeDtypeStruct((rows, cols), f32),
            jax.ShapeDtypeStruct((taps, channels), f32),
            jax.ShapeDtypeStruct((rows, rank), bf16),
        ),
        in_specs=[pl.BlockSpec(memory_space=pl.ANY)] * 7,
        out_specs=(vmem,) * 3,
        scratch_shapes=[
            *(pltpu.VMEM(a.shape, a.dtype) for a in (x, v, g, c, f, m1, m2)),
            dma((7,)),
            pltpu.VMEM((m, tokens, cols), bf16),
            pltpu.VMEM((m, tokens, cols), bf16),
            pltpu.VMEM((m, rank, rank), f32),
            pltpu.VMEM((n, rows, cols), bf16),
            pltpu.VMEM((n, rows, cols), bf16),
            pltpu.VMEM((reach, channels), bf16),
            pltpu.VMEM((groups, reach + tokens, LANES), f32),
            pltpu.VMEM((groups, tokens, LANES), f32),
            pltpu.VMEM((groups * padded, LANES), f32),
            pltpu.VMEM((n, chunk, LANES), bf16),
            pltpu.VMEM((n, chunk, LANES), bf16),
            pltpu.VMEM((n, chunk, LANES), bf16),
            pltpu.VMEM((m, rows, cols), f32),
            dma((m,)),
            dma((m,)),
            dma((m,)),
            dma((m,)),
            dma((n,)),
            dma((n,)),
            dma,
            dma,
            dma((n,)),
            dma((n,)),
            dma((n,)),
            dma((n,)),
            dma((m,)),
            dma((m,)),
        ],
        compiler_params=pltpu.CompilerParams(collective_id=0, has_side_effects=True),
        name="reduce",
    )(x, v, g, c, f, m1, m2)

    steps = 4 if features % (4 * LANES) == 0 else 1
    operands = (dn, f, w, proj, m1, m2, kg, k, k1, k2)
    results = (
        jax.ShapeDtypeStruct(w.shape, f32),
        jax.ShapeDtypeStruct(w.shape, bf16),
        jax.ShapeDtypeStruct(w.shape, f32),
        jax.ShapeDtypeStruct(m1.shape, f32),
        jax.ShapeDtypeStruct(m1.shape, f32),
        jax.ShapeDtypeStruct(k.shape, f32),
        jax.ShapeDtypeStruct(k.shape, f32),
        jax.ShapeDtypeStruct(k.shape, f32),
    )
    hbm = pl.BlockSpec(memory_space=pl.ANY)
    return pl.pallas_call(
        functools.partial(update_kernel, steps),
        out_shape=results,
        in_specs=[hbm] * 10,
        out_specs=(hbm,) * 8,
        scratch_shapes=[
            *(pltpu.VMEM(a.shape, a.dtype) for a in operands),
            *(pltpu.VMEM(a.shape, a.dtype) for a in results),
            dma((10,)),
            dma((steps,)),
            dma((steps,)),
            dma((8,)),
            dma((3, steps)),
        ],
        name="update",
    )(*operands)


def solution(mesh):
    both, rows, cols = P("fs", "tp"), P("fs", None), P(None, "tp")
    return jax.shard_map(
        functools.partial(body, mesh.shape["fs"], mesh.shape["tp"]),
        mesh=mesh,
        in_specs=(both, rows, both, both, P("tp", None), both, both, both, cols, cols, cols),
        out_specs=(both, both, both, both, both, cols, cols, cols),
        check_vma=False,
    )
```

profile of v0, /device:TPU:0, one launch (start us, length us, event | category | flops | bytes accessed | tf_op | source)
XLA Modules:
  0.0 33.7 jit_solution(12617890469747969151)
XLA Ops:
  0.6 29.5 %reduce.1 = (f32[128,128]{1,0:T(8,128)}, f32[31,1024]{1,0:T(8,128)}, bf16[128,256]{1,0:T(8,128)(2,1)}) custom-call(bf16[128,2048]{1,0:T(8,128)(2,1)} %x_hbm.1, bf16[128,2048]{1,0:T(8,128)(2,1)} %v_hbm.1, bf16[128,1024]{1,0:T(8,128)(2,1)} %g_hbm.1, bf16[128,1024]{1,0:T(8,128)(2,1)} %c_hbm.1, bf16[2048,256]{1,0:T(8,128)(2,1)} %refs_1_.1, f32[128,128]{1,0:T(8,128)} %refs_4_.1, ...), custom_call_target="tpu_custom_call" | custom-call | tf_op jit(solution)/shard_map/reduce/pallas_call | solution.py:309
  30.1 3.5 %update.1 = (f32[128,2048]{1,0:T(8,128)}, bf16[128,2048]{1,0:T(8,128)(2,1)}, f32[128,2048]{1,0:T(8,128)}, f32[128,128]{1,0:T(8,128)}, f32[128,128]{1,0:T(8,128)}...) custom-call(bf16[128,256]{1,0:T(8,128)(2,1)} %get-tuple-element.11.refs_0_, ...), custom_call_target="tpu_custom_call" | custom-call | tf_op jit(solution)/shard_map/update/pallas_call | solution.py:366
where the time goes:
time: 33.8 us; the launch traced here: 33.7 us
  Pallas kernels  33 us (98%)
  between operations  0.64 us (2%)
    pallas_call x1, Pallas kernels, body(): pl.pallas_call(functools.partial(reduce_kernel, n, m), out_shape=(jax.Sha...  29.5 us
    pallas_call x1, Pallas kernels, body(): pl.pallas_call(functools.partial(update_kernel, steps), out_shape=results...  3.53 us

commit v1 on v0

v1 whole, which is shorter than its diff:
```python
import functools
import types

import jax
import jax.numpy as jnp
from jax import lax
from jax.experimental import pallas as pl
from jax.experimental.pallas import tpu as pltpu
from jax.sharding import PartitionSpec as P

MESH = pl.DeviceIdType.MESH
LANES = 128
SUBLANES = 8
f32 = jnp.float32
bf16 = jnp.bfloat16
FIRST = (((0,), (0,)), ((), ()))
LAST = (((1,), (1,)), ((), ()))


def factors(n):
    lo = max(d for d in range(1, n + 1) if n % d == 0 and d * d <= n)
    return n // lo, lo


def steps_of(features):
    return 4 if features % (4 * LANES) == 0 else 1


def remote(src, dst, send, recv, axis, peer):
    return pltpu.make_async_remote_copy(
        src_ref=src,
        dst_ref=dst,
        send_sem=send,
        recv_sem=recv,
        device_id={axis: peer},
        device_id_type=MESH,
    )


def column_sums(values):
    row = lax.broadcasted_iota(jnp.int32, (SUBLANES, LANES), 0)
    blocks = []
    for at in range(0, len(values), SUBLANES):
        level, bit = values[at : at + SUBLANES], 1
        while len(level) > 1:
            low = (row & bit) == 0
            level = [
                jnp.where(low, a, b) + pltpu.roll(jnp.where(low, b, a), bit, 0)
                for a, b in zip(level[::2], level[1::2])
            ]
            bit *= 2
        blocks.append(level[0])
    return jnp.concatenate(blocks, axis=0)


def reduce_kernel(names, n, m, hi, lo, *refs):
    (x_hbm, v_hbm, g_hbm, c_hbm, f_hbm, w_hbm, m1_hbm, m2_hbm, k_hbm, k1_hbm, k2_hbm) = refs[:11]
    (dir_ref, gh_ref, gl_ref, f_ref, w_ref, n1_ref, n2_ref, nk_ref, nk1_ref, nk2_ref) = refs[11:21]
    s = types.SimpleNamespace(**dict(zip(names, refs[21:])))
    me = lax.axis_index("fs")
    my = lax.axis_index("tp")
    h, l = me // lo, lax.rem(me, lo)
    tokens, features = s.x.shape
    rows, cols = s.m1.shape
    reach = s.halo.shape[0]
    groups = s.ext.shape[0]
    taps = nk_ref.shape[0]
    padded = s.stage.shape[0] // groups
    piece = tokens // m
    steps = steps_of(features)
    block = features // steps
    copy = pltpu.make_async_copy

    def lo_peer(off):
        return lax.rem(l + off, lo)

    def lo_from(off):
        return lax.rem(l + lo - off, lo)

    def hi_peer(off):
        return lax.rem(h + off, hi)

    def hi_from(off):
        return lax.rem(h + hi - off, hi)

    def peers(count, own, fn):
        def step(off, carry):
            fn(off, lax.rem(own + off, count))
            return carry

        lax.fori_loop(1, count, step, 0)

    barrier = pltpu.get_barrier_semaphore()

    def hello(axis, peer):
        pl.semaphore_signal(barrier, inc=1, device_id={axis: peer}, device_id_type=MESH)

    for off in range(1, hi):
        hello("fs", hi_peer(off) * lo + l)
    for off in range(1, lo):
        hello("fs", h * lo + lo_peer(off))

    @pl.when(me + 1 < n)
    def _():
        hello("fs", me + 1)

    @pl.when(me > 0)
    def _():
        hello("fs", me - 1)

    for off in range(1, m):
        hello("tp", lax.rem(my + off, m))

    spans = [pl.ds(i * block, block) for i in range(steps)]
    x_in = [copy(x_hbm.at[:, at], s.x.at[:, at], s.x_s.at[i]) for i, at in enumerate(spans)]
    f_in = [copy(f_hbm.at[at], f_ref.at[at], s.f_s.at[i]) for i, at in enumerate(spans)]
    for i in range(steps):
        x_in[i].start()
        f_in[i].start()
    aligned = rows % LANES == 0
    if aligned:
        v_in = [
            copy(
                v_hbm.at[:, pl.ds(j * rows, rows)],
                s.v_src.at[j % lo, :, pl.ds(j // lo * rows, rows)],
                s.v_in.at[j],
            )
            for j in range(n)
        ]
    else:
        v_in = [copy(v_hbm, s.v_all, s.v_in.at[0])]
    for load in v_in:
        load.start()
    g_in = copy(g_hbm, s.g, s.small.at[0])
    c_in = copy(c_hbm, s.c, s.small.at[1])
    g_in.start()
    c_in.start()

    low = None
    for i, at in enumerate(spans):
        x_in[i].wait()
        f_in[i].wait()
        product = jnp.dot(s.x[:, at], f_ref[at, :], preferred_element_type=f32)
        low = product if low is None else low + product
    low = low.astype(bf16)
    for j in range(m):
        s.low_out[j] = low[:, j * cols : (j + 1) * cols]
    for load in v_in:
        load.wait()
    if not aligned:
        for j in range(n):
            s.v_src[j % lo, :, j // lo * rows : (j // lo + 1) * rows] = s.v_all[:, j * rows : (j + 1) * rows]
    g_in.wait()
    c_in.wait()

    greeted = (hi - 1) + (lo - 1) + (m - 1)
    greeted = greeted + jnp.where(me + 1 < n, 1, 0) + jnp.where(me > 0, 1, 0)
    pl.semaphore_wait(barrier, greeted)

    low_copies = [
        remote(
            s.low_out.at[lax.rem(my + off, m)],
            s.low_in.at[my],
            s.low_s.at[off],
            s.low_r.at[off],
            "tp",
            lax.rem(my + off, m),
        )
        for off in range(1, m)
    ]
    for one in low_copies:
        one.start()
    s.low_in[my] = s.low_out[my]

    halo_copy = remote(
        s.g.at[pl.ds(tokens - reach, reach)], s.halo, s.halo_s, s.halo_r, "fs", lax.rem(me + 1, n)
    )

    @pl.when(me + 1 < n)
    def _():
        halo_copy.start()

    share = pl.ds(my * piece, piece)
    v_copies = [
        remote(
            s.v_src.at[lo_peer(off), share],
            s.v_got.at[l, share],
            s.v_s.at[off],
            s.v_r.at[off],
            "fs",
            h * lo + lo_peer(off),
        )
        for off in range(1, lo)
    ]
    for one in v_copies:
        one.start()

    for off in range(1, hi):
        pl.semaphore_signal(
            s.ready, inc=1, device_id={"fs": hi_peer(off) * lo + l}, device_id_type=MESH
        )

    late = [(w_hbm, w_ref), (m1_hbm, s.m1), (m2_hbm, s.m2), (k_hbm, s.k), (k1_hbm, s.k1), (k2_hbm, s.k2)]
    late = [copy(a, b, s.small.at[2 + i]) for i, (a, b) in enumerate(late)]
    for load in late:
        load.start()

    for g in range(groups):
        lanes = slice(g * LANES, (g + 1) * LANES)
        s.ext[g, :reach] = jnp.zeros((reach, LANES), f32)
        s.ext[g, reach:] = s.g[:, lanes].astype(f32)
        s.cot[g] = s.c[:, lanes].astype(f32)

    def group_step(count, add):
        def step(g, carry):
            right = s.cot[g, :count, :]
            sums = []
            for k in range(taps):
                product = s.ext[g, pl.ds(reach - k, count), :] * right
                sums.append(jnp.sum(product.reshape(count // SUBLANES, SUBLANES, LANES), axis=0))
            sums += [jnp.zeros((SUBLANES, LANES), f32)] * (padded - taps)
            at = pl.ds(pl.multiple_of(g * padded, padded), padded)
            total = column_sums(sums)
            s.stage[at, :] = s.stage[at, :] + total if add else total
            return carry

        return step

    early = groups // 2
    lax.fori_loop(0, early, group_step(tokens, False), 0)

    for one in low_copies:
        one.wait()
    reduced = s.low_in[0].astype(f32)
    for j in range(1, m):
        reduced = reduced + s.low_in[j].astype(f32)
    s.turned[l] = reduced.T.astype(bf16)
    turn_copies = [
        remote(
            s.turned.at[l],
            s.turned.at[l],
            s.turn_s.at[off],
            s.turn_r.at[off],
            "fs",
            h * lo + lo_peer(off),
        )
        for off in range(1, lo)
    ]
    for one in turn_copies:
        one.start()

    lax.fori_loop(early, groups, group_step(tokens, False), 0)

    @pl.when(me > 0)
    def _():
        halo_copy.wait_recv()

    @pl.when(me == 0)
    def _():
        s.halo[...] = jnp.zeros(s.halo.shape, bf16)

    halo_f = s.halo[...].astype(f32)
    for g in range(groups):
        s.ext[g, :reach] = halo_f[:, g * LANES : (g + 1) * LANES]
        s.ext[g, reach : 2 * reach] = jnp.zeros((reach, LANES), f32)
    lax.fori_loop(0, groups, group_step(reach, True), 0)
    s.tap_out[...] = s.stage[...].reshape(s.tap_out.shape).astype(bf16)

    pl.semaphore_wait(s.ready, hi - 1)

    def tap_copy(off, p):
        return remote(s.tap_out.at[p], s.tap_in.at[me], s.tap_s.at[off], s.tap_r.at[off], "fs", p)

    peers(n, me, lambda off, p: tap_copy(off, p).start())
    s.tap_in[me] = s.tap_out[me]

    forwards = []
    for off in range(1, lo):
        v_copies[off - 1].wait_recv()
        at = s.v_got.at[lo_from(off), share]
        for t in range(1, m):
            one = remote(at, at, s.pass_s.at[off, t], s.pass_r.at[off, t], "tp", lax.rem(my + t, m))
            one.start()
            forwards.append(one)

    acc = jnp.dot(s.turned[l], s.v_src[l], preferred_element_type=f32)
    for off in range(1, lo):
        for t in range(1, m):
            forwards[(off - 1) * (m - 1) + t - 1].wait_recv()
        turn_copies[off - 1].wait_recv()
        p = lo_from(off)
        acc = acc + jnp.dot(s.turned[p], s.v_got[p], preferred_element_type=f32)
    for q in range(hi):
        mine = acc[:, q * rows : (q + 1) * rows]
        s.part[q] = mine
        s.bulk_out[q] = mine.astype(bf16)
    bulk_copies = [
        remote(
            s.bulk_out.at[hi_peer(off)],
            s.bulk_in.at[h],
            s.bulk_s.at[off],
            s.bulk_r.at[off],
            "fs",
            hi_peer(off) * lo + l,
        )
        for off in range(1, hi)
    ]
    for one in bulk_copies:
        one.start()

    s.gram[my] = lax.dot_general(f_ref[...], f_ref[...], FIRST, preferred_element_type=f32)
    gram_copies = [
        remote(s.gram.at[my], s.gram.at[my], s.gram_s.at[off], s.gram_r.at[off], "tp", lax.rem(my + off, m))
        for off in range(1, m)
    ]
    for one in gram_copies:
        one.start()

    peers(n, me, lambda off, p: tap_copy(off, p).wait())
    s.tap_all[me] = jnp.sum(s.tap_in[...].astype(f32), axis=0).astype(bf16)

    def all_copy(off, p):
        return remote(s.tap_all.at[me], s.tap_all.at[me], s.all_s.at[off], s.all_r.at[off], "fs", p)

    peers(n, me, lambda off, p: all_copy(off, p).start())

    for one in gram_copies:
        one.wait()
    total = s.gram[0]
    for j in range(1, m):
        total = total + s.gram[j]
    top = total.astype(bf16)
    gh_ref[...] = top
    gl_ref[...] = (total - top.astype(f32)).astype(bf16)
    for load in late:
        load.wait()

    projected = s.part[h]
    for off in range(1, hi):
        bulk_copies[off - 1].wait_recv()
        projected = projected + s.bulk_in[hi_from(off)].astype(f32)
    projected = projected.T
    first = 0.8 * s.m1[...] + 0.2 * projected
    second = 0.9 * s.m2[...] + 0.1 * projected * projected
    s.dirs[my] = (first * lax.rsqrt(second)).astype(bf16)
    dir_copies = [
        remote(s.dirs.at[my], s.dirs.at[my], s.dir_s.at[off], s.dir_r.at[off], "tp", lax.rem(my + off, m))
        for off in range(1, m)
    ]
    for one in dir_copies:
        one.start()
    n1_ref[...] = first
    n2_ref[...] = second

    peers(n, me, lambda off, p: all_copy(off, p).wait())
    s.stage[...] = s.tap_all[...].astype(f32).reshape(s.stage.shape)
    for g in range(groups):
        lanes = slice(g * LANES, (g + 1) * LANES)
        grad = s.stage[g * padded : g * padded + taps, :]
        first = 0.8 * s.k1[:, lanes] + 0.2 * grad
        second = 0.9 * s.k2[:, lanes] + 0.1 * grad * grad
        nk1_ref[:, lanes] = first
        nk2_ref[:, lanes] = second
        nk_ref[:, lanes] = s.k[:, lanes] - 0.05 * first * lax.rsqrt(second)

    @pl.when(me + 1 < n)
    def _():
        halo_copy.wait_send()

    for one in v_copies + forwards + turn_copies + bulk_copies:
        one.wait_send()
    for one in dir_copies:
        one.wait()
    for j in range(m):
        dir_ref[:, j * cols : (j + 1) * cols] = s.dirs[j]


def update_kernel(steps, width, *refs):
    dir_ref, gh_ref, gl_ref, f_ref, w_ref = refs[:5]
    small, target, made = refs[5:10], refs[10:18], refs[18:21]
    small_s, wide_s = refs[21:]
    value_ref, copy_ref, step_ref = made
    copy = pltpu.make_async_copy
    outs = [copy(small[j], target[3 + j], small_s.at[j]) for j in range(5)]
    for out in outs:
        out.start()
    direction = dir_ref[...]
    turned = jnp.dot(direction, gh_ref[...], preferred_element_type=f32)
    turned = turned + jnp.dot(direction, gl_ref[...], preferred_element_type=f32)
    mean = jnp.sum(turned * direction.astype(f32), axis=1, keepdims=True) / width
    scale = lax.rsqrt(mean + 0.01)
    block = f_ref.shape[0] // steps
    for i in range(steps):
        at = pl.ds(i * block, block)
        step = lax.dot_general(direction, f_ref[at, :], LAST, preferred_element_type=f32) * scale
        step_ref[:, at] = step
        value = w_ref[:, at] - 0.05 * step
        value_ref[:, at] = value
        copy_ref[:, at] = value.astype(bf16)
        for j in range(3):
            out = copy(made[j].at[:, at], target[j].at[:, at], wide_s.at[j, i])
            out.start()
            outs.append(out)
    for out in outs:
        out.wait()


def body(n, m, x, v, g, c, f, w, m1, m2, k, k1, k2):
    tokens = x.shape[0]
    features, rank = f.shape
    rows, cols = m1.shape
    taps, channels = k.shape
    hi, lo = factors(n)
    groups = channels // LANES
    reach = -(-(taps - 1) // 16) * 16
    padded = -(-taps // SUBLANES) * SUBLANES
    chunk = groups * padded // n
    steps = steps_of(features)
    vmem, dma = pltpu.VMEM, pltpu.SemaphoreType.DMA
    scratch = dict(
        x=vmem(x.shape, x.dtype),
        v_all=vmem(v.shape if rows % LANES else (16, LANES), bf16),
        v_src=vmem((lo, tokens, hi * rows), bf16),
        v_got=vmem((lo, tokens, hi * rows), bf16),
        g=vmem(g.shape, g.dtype),
        c=vmem(c.shape, c.dtype),
        m1=vmem(m1.shape, f32),
        m2=vmem(m2.shape, f32),
        k=vmem(k.shape, f32),
        k1=vmem(k.shape, f32),
        k2=vmem(k.shape, f32),
        low_out=vmem((m, tokens, cols), bf16),
        low_in=vmem((m, tokens, cols), bf16),
        turned=vmem((lo, cols, tokens), bf16),
        gram=vmem((m, rank, rank), f32),
        part=vmem((hi, cols, rows), f32),
        bulk_out=vmem((hi, cols, rows), bf16),
        bulk_in=vmem((hi, cols, rows), bf16),
        halo=vmem((reach, channels), bf16),
        ext=vmem((groups, reach + tokens, LANES), f32),
        cot=vmem((groups, tokens, LANES), f32),
        stage=vmem((groups * padded, LANES), f32),
        tap_out=vmem((n, chunk, LANES), bf16),
        tap_in=vmem((n, chunk, LANES), bf16),
        tap_all=vmem((n, chunk, LANES), bf16),
        dirs=vmem((m, rows, cols), bf16),
        ready=pltpu.SemaphoreType.REGULAR,
        x_s=dma((steps,)),
        f_s=dma((steps,)),
        v_in=dma((n,)),
        small=dma((8,)),
        low_s=dma((m,)),
        low_r=dma((m,)),
        halo_s=dma,
        halo_r=dma,
        v_s=dma((lo,)),
        v_r=dma((lo,)),
        pass_s=dma((lo, m)),
        pass_r=dma((lo, m)),
        turn_s=dma((lo,)),
        turn_r=dma((lo,)),
        bulk_s=dma((hi,)),
        bulk_r=dma((hi,)),
        gram_s=dma((m,)),
        gram_r=dma((m,)),
        tap_s=dma((n,)),
        tap_r=dma((n,)),
        all_s=dma((n,)),
        all_r=dma((n,)),
        dir_s=dma((m,)),
        dir_r=dma((m,)),
    )
    inputs = (x, v, g, c, f, w, m1, m2, k, k1, k2)
    inputs = [pltpu.with_memory_space_constraint(a, pltpu.HBM) for a in inputs]
    shape = jax.ShapeDtypeStruct
    between = (
        shape((rows, rank), bf16),
        shape((rank, rank), bf16),
        shape((rank, rank), bf16),
        shape(f.shape, bf16),
        shape(w.shape, f32),
        shape(m1.shape, f32),
        shape(m1.shape, f32),
        shape(k.shape, f32),
        shape(k.shape, f32),
        shape(k.shape, f32),
    )
    hbm = pl.BlockSpec(memory_space=pltpu.HBM)
    held = pl.BlockSpec(memory_space=pltpu.VMEM)
    results = pl.pallas_call(
        functools.partial(reduce_kernel, tuple(scratch), n, m, hi, lo),
        out_shape=between,
        in_specs=[hbm] * len(inputs),
        out_specs=(held,) * len(between),
        scratch_shapes=list(scratch.values()),
        compiler_params=pltpu.CompilerParams(
            collective_id=0, has_side_effects=True, vmem_limit_bytes=24 << 20
        ),
        name="reduce",
    )(*inputs)

    outputs = (
        shape(w.shape, f32),
        shape(w.shape, bf16),
        shape(w.shape, f32),
        shape(m1.shape, f32),
        shape(m1.shape, f32),
        shape(k.shape, f32),
        shape(k.shape, f32),
        shape(k.shape, f32),
    )
    return pl.pallas_call(
        functools.partial(update_kernel, steps, features * m),
        out_shape=outputs,
        in_specs=[held] * len(between),
        out_specs=(hbm,) * len(outputs),
        scratch_shapes=[
            vmem(w.shape, f32),
            vmem(w.shape, bf16),
            vmem(w.shape, f32),
            dma((5,)),
            dma((3, steps)),
        ],
        compiler_params=pltpu.CompilerParams(vmem_limit_bytes=24 << 20),
        name="update",
    )(*results)


def solution(mesh):
    both, rows, cols = P("fs", "tp"), P("fs", None), P(None, "tp")
    return jax.shard_map(
        functools.partial(body, mesh.shape["fs"], mesh.shape["tp"]),
        mesh=mesh,
        in_specs=(both, rows, both, both, P("tp", None), both, both, both, cols, cols, cols),
        out_specs=(both, both, both, both, both, cols, cols, cols),
        check_vma=False,
    )
```

time: 33.8 us -> 24.9 us (0.74)
  Pallas kernels: 33 us -> 24.1 us
    pallas_call x2, Pallas kernels: 33 us -> 24.1 us  [the longest x1 21.9 us: body(): pl.pallas_call(functools.partial(reduce_kernel, tuple(scratch), n, m, hi,...]
where the time goes in v1:
time: 24.9 us; the launch traced here: 24.7 us
  Pallas kernels  24.1 us (97%)
  between operations  0.65 us (3%)
    pallas_call x1, Pallas kernels, body(): pl.pallas_call(functools.partial(reduce_kernel, tuple(scratch), n, m, hi,...  21.9 us
    pallas_call x1, Pallas kernels, body(): pl.pallas_call(functools.partial(update_kernel, steps, features * m), out...  2.15 us

profile of v1, /device:TPU:0, one launch (start us, length us, event | category | flops | bytes accessed | tf_op | source)
XLA Modules:
  0.0 24.7 jit_solution(13324949366506416246)
XLA Ops:
  0.6 21.9 %reduce.1 = (bf16[128,256]{1,0:T(8,128)(2,1)S(1)}, bf16[256,256]{1,0:T(8,128)(2,1)S(1)}, bf16[256,256]{1,0:T(8,128)(2,1)S(1)}, bf16[2048,256]{1,0:T(8,128)(2,1)S...) custom-call(bf16[128,2048]{1,0:T(8,128)(2,1)} %refs_0_.1, ...), custom_call_target="tpu_custom_call" | custom-call | tf_op jit(solution)/shard_map/reduce/pallas_call | solution.py:490
  22.6 2.1 %update.1 = (f32[128,2048]{1,0:T(8,128)}, bf16[128,2048]{1,0:T(8,128)(2,1)}, f32[128,2048]{1,0:T(8,128)}, f32[128,128]{1,0:T(8,128)}, f32[128,128]{1,0:T(8,128)}...) custom-call(bf16[128,256]{1,0:T(8,128)(2,1)S(1)} %get-tuple-element.18.refs_0_, ...), custom_call_target="tpu_custom_call" | custom-call | tf_op jit(solution)/shard_map/update/pallas_call | solution.py:512

commit v2 on v1

v2 whole, which is shorter than its diff:
```python
import functools
import types

import jax
import jax.numpy as jnp
from jax import lax
from jax.experimental import pallas as pl
from jax.experimental.pallas import tpu as pltpu
from jax.sharding import PartitionSpec as P

MESH = pl.DeviceIdType.MESH
LANES = 128
SUBLANES = 8
f32 = jnp.float32
bf16 = jnp.bfloat16
FIRST = (((0,), (0,)), ((), ()))
LAST = (((1,), (1,)), ((), ()))


def factors(n):
    lo = max(d for d in range(1, n + 1) if n % d == 0 and d * d <= n)
    return n // lo, lo


def steps_of(features):
    return 4 if features % (4 * LANES) == 0 else 1


def remote(src, dst, send, recv, axis, peer):
    return pltpu.make_async_remote_copy(
        src_ref=src,
        dst_ref=dst,
        send_sem=send,
        recv_sem=recv,
        device_id={axis: peer},
        device_id_type=MESH,
    )


def column_sums(values):
    row = lax.broadcasted_iota(jnp.int32, (SUBLANES, LANES), 0)
    blocks = []
    for at in range(0, len(values), SUBLANES):
        level, bit = values[at : at + SUBLANES], 1
        while len(level) > 1:
            low = (row & bit) == 0
            level = [
                jnp.where(low, a, b) + pltpu.roll(jnp.where(low, b, a), bit, 0)
                for a, b in zip(level[::2], level[1::2])
            ]
            bit *= 2
        blocks.append(level[0])
    return jnp.concatenate(blocks, axis=0)


def landed(ref, sem):
    pltpu.make_async_copy(ref, ref, sem).wait()


def reduce_kernel(names, n, m, hi, lo, *refs):
    (x_hbm, v_hbm, g_hbm, c_hbm, f_hbm, w_hbm, m1_hbm, m2_hbm, k_hbm, k1_hbm, k2_hbm) = refs[:11]
    (dir_ref, gh_ref, gl_ref, f_ref, w_ref, n1_ref, n2_ref, nk_ref, nk1_ref, nk2_ref) = refs[11:21]
    s = types.SimpleNamespace(**dict(zip(names, refs[21:])))
    me = lax.axis_index("fs")
    my = lax.axis_index("tp")
    h, l = me // lo, lax.rem(me, lo)
    half = hi // 2
    near = h // half * half
    far = half - near
    spot = me - near * lo
    tokens, features = s.x.shape
    rows, cols = s.m.shape[1:]
    reach = s.halo.shape[0]
    groups = s.ext.shape[0]
    taps = nk_ref.shape[0]
    padded = s.stage.shape[0] // groups
    piece = tokens // m
    steps = steps_of(features)
    block = features // steps
    copy = pltpu.make_async_copy

    def lo_peer(off):
        return lax.rem(l + off, lo)

    def lo_from(off):
        return lax.rem(l + lo - off, lo)

    def peers(count, own, fn):
        def step(off, carry):
            fn(off, lax.rem(own + off, count))
            return carry

        lax.fori_loop(1, count, step, 0)

    spans = [pl.ds(i * block, block) for i in range(steps)]
    x_in = [copy(x_hbm.at[:, at], s.x.at[:, at], s.x_s.at[i]) for i, at in enumerate(spans)]
    f_in = [copy(f_hbm.at[at], f_ref.at[at], s.f_s.at[i]) for i, at in enumerate(spans)]
    for i in range(steps):
        x_in[i].start()
        f_in[i].start()

    barrier = pltpu.get_barrier_semaphore()

    def hello(axis, peer):
        pl.semaphore_signal(barrier, inc=1, device_id={axis: peer}, device_id_type=MESH)

    for off in range(1, hi):
        hello("fs", lax.rem(h + off, hi) * lo + l)
    for off in range(1, lo):
        hello("fs", h * lo + lo_peer(off))

    @pl.when(me + 1 < n)
    def _():
        hello("fs", me + 1)

    @pl.when(me > 0)
    def _():
        hello("fs", me - 1)

    for off in range(1, m):
        hello("tp", lax.rem(my + off, m))

    width = half * lo * rows
    near_at = pl.ds(pl.multiple_of(near * lo * rows, width), width)
    far_at = pl.ds(pl.multiple_of(far * lo * rows, width), width)
    aligned = rows % LANES == 0
    if aligned:
        for i in range(half):
            for p in range(lo):
                start = pl.multiple_of((far + i) * lo * rows + p * rows, rows)
                copy(
                    v_hbm.at[:, pl.ds(start, rows)],
                    s.v_far.at[p, :, pl.ds(i * rows, rows)],
                    s.v_in.at[0],
                ).start()
    else:
        copy(v_hbm.at[:, far_at], s.v_all, s.v_in.at[0]).start()
    g_in = copy(g_hbm, s.g, s.g_s)
    c_in = copy(c_hbm, s.c, s.c_s)
    v_in = copy(v_hbm.at[:, near_at], s.v_near, s.v_in.at[1])
    g_in.start()
    c_in.start()
    v_in.start()

    low = None
    for i, at in enumerate(spans):
        x_in[i].wait()
        f_in[i].wait()
        product = jnp.dot(s.x[:, at], f_ref[at, :], preferred_element_type=f32)
        low = product if low is None else low + product
    low = low.astype(bf16)
    for j in range(m):
        s.low_out[j] = low[:, j * cols : (j + 1) * cols]
    if aligned:
        landed(s.v_far, s.v_in.at[0])
    else:
        landed(s.v_all, s.v_in.at[0])
        for i in range(half):
            for p in range(lo):
                at = (i * lo + p) * rows
                s.v_far[p, :, i * rows : (i + 1) * rows] = s.v_all[:, at : at + rows]
    g_in.wait()
    c_in.wait()

    greeted = (hi - 1) + (lo - 1) + (m - 1)
    greeted = greeted + jnp.where(me + 1 < n, 1, 0) + jnp.where(me > 0, 1, 0)
    pl.semaphore_wait(barrier, greeted)

    for off in range(1, m):
        p = lax.rem(my + off, m)
        remote(s.low_out.at[p], s.low_in.at[my], s.low_s, s.low_r, "tp", p).start()
    s.low_in[my] = s.low_out[my]

    halo_copy = remote(
        s.g.at[pl.ds(tokens - reach, reach)], s.halo, s.halo_s, s.halo_r, "fs", lax.rem(me + 1, n)
    )

    @pl.when(me + 1 < n)
    def _():
        halo_copy.start()

    share = pl.ds(my * piece, piece)
    v_copies = [
        remote(
            s.v_far.at[lo_peer(off), share],
            s.v_got.at[l, share],
            s.v_s,
            s.v_r.at[off - 1],
            "fs",
            h * lo + lo_peer(off),
        )
        for off in range(1, lo)
    ]
    for one in v_copies:
        one.start()

    for off in range(1, hi):
        pl.semaphore_signal(
            s.ready,
            inc=1,
            device_id={"fs": lax.rem(h + off, hi) * lo + l},
            device_id_type=MESH,
        )

    w_in = copy(w_hbm, w_ref, s.w_s)
    w_in.start()
    for i, ref in enumerate((m1_hbm, m2_hbm)):
        copy(ref, s.m.at[i], s.m_s).start()
    for i, ref in enumerate((k_hbm, k1_hbm, k2_hbm)):
        copy(ref, s.k.at[i], s.k_s).start()

    for g in range(groups):
        lanes = slice(g * LANES, (g + 1) * LANES)
        s.ext[g, :reach] = jnp.zeros((reach, LANES), f32)
        s.ext[g, reach:] = s.g[:, lanes].astype(f32)
        s.cot[g] = s.c[:, lanes].astype(f32)

    def group_step(count, add):
        def step(g, carry):
            right = s.cot[g, :count, :]
            sums = []
            for k in range(taps):
                product = s.ext[g, pl.ds(reach - k, count), :] * right
                sums.append(jnp.sum(product.reshape(count // SUBLANES, SUBLANES, LANES), axis=0))
            sums += [jnp.zeros((SUBLANES, LANES), f32)] * (padded - taps)
            at = pl.ds(pl.multiple_of(g * padded, padded), padded)
            total = column_sums(sums)
            s.stage[at, :] = s.stage[at, :] + total if add else total
            return carry

        return step

    early = groups // 2
    lax.fori_loop(0, early, group_step(tokens, False), 0)

    landed(s.low_in.at[pl.ds(0, m - 1)], s.low_r)
    reduced = s.low_in[0].astype(f32)
    for j in range(1, m):
        reduced = reduced + s.low_in[j].astype(f32)
    turned = reduced.T.astype(bf16)
    s.turned[l] = turned
    turn_copies = [
        remote(
            s.turned.at[l],
            s.turned.at[l],
            s.turn_s,
            s.turn_r.at[off - 1],
            "fs",
            h * lo + lo_peer(off),
        )
        for off in range(1, lo)
    ]
    for one in turn_copies:
        one.start()

    lax.fori_loop(early, groups, group_step(tokens, False), 0)

    v_in.wait()
    direct = jnp.dot(turned, s.v_near[...], preferred_element_type=f32)
    for j in range(half * lo):
        s.near_out[j] = direct[:, j * rows : (j + 1) * rows].astype(bf16)

    @pl.when(me > 0)
    def _():
        halo_copy.wait_recv()

    @pl.when(me == 0)
    def _():
        s.halo[...] = jnp.zeros(s.halo.shape, bf16)

    halo_f = s.halo[...].astype(f32)
    for g in range(groups):
        s.ext[g, :reach] = halo_f[:, g * LANES : (g + 1) * LANES]
        s.ext[g, reach : 2 * reach] = jnp.zeros((reach, LANES), f32)
    lax.fori_loop(0, groups, group_step(reach, True), 0)
    s.tap_out[...] = s.stage[...].reshape(s.tap_out.shape).astype(bf16)

    pl.semaphore_wait(s.ready, hi - 1)

    def send_taps(off, p):
        remote(s.tap_out.at[p], s.tap_in.at[me], s.tap_s, s.tap_r, "fs", p).start()

    peers(n, me, send_taps)
    s.tap_in[me] = s.tap_out[me]

    def send_near(off, p):
        remote(s.near_out.at[p], s.near_in.at[spot], s.near_s, s.near_r, "fs", near * lo + p).start()

    peers(half * lo, spot, send_near)
    s.near_in[spot] = s.near_out[spot]

    for off in range(1, lo):
        v_copies[off - 1].wait_recv()
        at = s.v_got.at[lo_from(off), share]
        for t in range(1, m):
            remote(at, at, s.pass_s, s.pass_r.at[off - 1], "tp", lax.rem(my + t, m)).start()

    acc = jnp.dot(s.turned[l], s.v_far[l], preferred_element_type=f32)
    for off in range(1, lo):
        p = lo_from(off)
        landed(s.v_got.at[p, pl.ds(0, tokens - piece)], s.pass_r.at[off - 1])
        turn_copies[off - 1].wait_recv()
        acc = acc + jnp.dot(s.turned[p], s.v_got[p], preferred_element_type=f32)
    for i in range(half):
        s.far_out[i] = acc[:, i * rows : (i + 1) * rows].astype(bf16)
    for i in range(half):
        remote(
            s.far_out.at[i], s.far_in.at[h - near], s.far_s, s.far_r, "fs", (far + i) * lo + l
        ).start()

    s.gram[my] = lax.dot_general(f_ref[...], f_ref[...], FIRST, preferred_element_type=f32)
    for off in range(1, m):
        remote(s.gram.at[my], s.gram.at[my], s.gram_s, s.gram_r, "tp", lax.rem(my + off, m)).start()

    landed(s.tap_in.at[pl.ds(0, n - 1)], s.tap_r)
    s.tap_all[me] = jnp.sum(s.tap_in[...].astype(f32), axis=0).astype(bf16)

    def send_all(off, p):
        remote(s.tap_all.at[me], s.tap_all.at[me], s.all_s, s.all_r, "fs", p).start()

    peers(n, me, send_all)

    landed(s.gram.at[pl.ds(0, m - 1)], s.gram_r)
    total = s.gram[0]
    for j in range(1, m):
        total = total + s.gram[j]
    top = total.astype(bf16)
    gh_ref[...] = top
    gl_ref[...] = (total - top.astype(f32)).astype(bf16)
    w_in.wait()
    landed(s.m, s.m_s)
    landed(s.k, s.k_s)

    landed(s.near_in.at[pl.ds(0, half * lo - 1)], s.near_r)
    projected = s.near_in[0].astype(f32)
    for j in range(1, half * lo):
        projected = projected + s.near_in[j].astype(f32)
    landed(s.far_in, s.far_r)
    for i in range(half):
        projected = projected + s.far_in[i].astype(f32)
    projected = projected.T
    first = 0.8 * s.m[0] + 0.2 * projected
    second = 0.9 * s.m[1] + 0.1 * projected * projected
    s.dirs[my] = (first * lax.rsqrt(second)).astype(bf16)
    for off in range(1, m):
        remote(s.dirs.at[my], s.dirs.at[my], s.dir_s, s.dir_r, "tp", lax.rem(my + off, m)).start()
    n1_ref[...] = first
    n2_ref[...] = second

    @pl.when(me + 1 < n)
    def _():
        halo_copy.wait_send()

    landed(s.low_out.at[pl.ds(0, m - 1)], s.low_s)
    landed(s.v_far.at[pl.ds(0, lo - 1), share], s.v_s)
    landed(s.v_far.at[pl.ds(0, lo - 1), pl.ds(0, tokens - piece)], s.pass_s)
    landed(s.turned.at[pl.ds(0, lo - 1)], s.turn_s)
    landed(s.near_out.at[pl.ds(0, half * lo - 1)], s.near_s)
    landed(s.far_out, s.far_s)
    landed(s.gram.at[pl.ds(0, m - 1)], s.gram_s)
    landed(s.tap_out.at[pl.ds(0, n - 1)], s.tap_s)
    landed(s.tap_all.at[pl.ds(0, n - 1)], s.all_s)

    landed(s.tap_all.at[pl.ds(0, n - 1)], s.all_r)
    s.stage[...] = s.tap_all[...].astype(f32).reshape(s.stage.shape)
    for g in range(groups):
        lanes = slice(g * LANES, (g + 1) * LANES)
        grad = s.stage[g * padded : g * padded + taps, :]
        first = 0.8 * s.k[1, :, lanes] + 0.2 * grad
        second = 0.9 * s.k[2, :, lanes] + 0.1 * grad * grad
        nk1_ref[:, lanes] = first
        nk2_ref[:, lanes] = second
        nk_ref[:, lanes] = s.k[0, :, lanes] - 0.05 * first * lax.rsqrt(second)

    landed(s.dirs.at[pl.ds(0, m - 1)], s.dir_s)
    landed(s.dirs.at[pl.ds(0, m - 1)], s.dir_r)
    for j in range(m):
        dir_ref[:, j * cols : (j + 1) * cols] = s.dirs[j]


def update_kernel(steps, width, *refs):
    dir_ref, gh_ref, gl_ref, f_ref, w_ref = refs[:5]
    small, target, made = refs[5:10], refs[10:18], refs[18:21]
    small_s, wide_s = refs[21:]
    value_ref, copy_ref, step_ref = made
    copy = pltpu.make_async_copy
    for j in range(5):
        copy(small[j], target[3 + j], small_s.at[j]).start()
    direction = dir_ref[...]
    turned = jnp.dot(direction, gh_ref[...], preferred_element_type=f32)
    turned = turned + jnp.dot(direction, gl_ref[...], preferred_element_type=f32)
    mean = jnp.sum(turned * direction.astype(f32), axis=1, keepdims=True) / width
    scale = lax.rsqrt(mean + 0.01)
    block = f_ref.shape[0] // steps
    for i in range(steps):
        at = pl.ds(i * block, block)
        step = lax.dot_general(direction, f_ref[at, :], LAST, preferred_element_type=f32) * scale
        step_ref[:, at] = step
        value = w_ref[:, at] - 0.05 * step
        value_ref[:, at] = value
        copy_ref[:, at] = value.astype(bf16)
        for j in range(3):
            copy(made[j].at[:, at], target[j].at[:, at], wide_s.at[j]).start()
    for j in range(5):
        copy(small[j], target[3 + j], small_s.at[j]).wait()
    for j in range(3):
        copy(made[j], target[j], wide_s.at[j]).wait()


def body(n, m, x, v, g, c, f, w, m1, m2, k, k1, k2):
    tokens = x.shape[0]
    features, rank = f.shape
    rows, cols = m1.shape
    taps, channels = k.shape
    hi, lo = factors(n)
    groups = channels // LANES
    reach = -(-(taps - 1) // 16) * 16
    padded = -(-taps // SUBLANES) * SUBLANES
    chunk = groups * padded // n
    steps = steps_of(features)
    vmem, dma = pltpu.VMEM, pltpu.SemaphoreType.DMA
    half = hi // 2
    width = half * lo * rows
    scratch = dict(
        x=vmem(x.shape, x.dtype),
        v_all=vmem((tokens, width) if rows % LANES else (16, LANES), bf16),
        v_near=vmem((tokens, width), bf16),
        v_far=vmem((lo, tokens, half * rows), bf16),
        v_got=vmem((lo, tokens, half * rows), bf16),
        g=vmem(g.shape, g.dtype),
        c=vmem(c.shape, c.dtype),
        m=vmem((2, rows, cols), f32),
        k=vmem((3, taps, channels), f32),
        low_out=vmem((m, tokens, cols), bf16),
        low_in=vmem((m, tokens, cols), bf16),
        turned=vmem((lo, cols, tokens), bf16),
        gram=vmem((m, rank, rank), f32),
        near_out=vmem((half * lo, cols, rows), bf16),
        near_in=vmem((half * lo, cols, rows), bf16),
        far_out=vmem((half, cols, rows), bf16),
        far_in=vmem((half, cols, rows), bf16),
        halo=vmem((reach, channels), bf16),
        ext=vmem((groups, reach + tokens, LANES), f32),
        cot=vmem((groups, tokens, LANES), f32),
        stage=vmem((groups * padded, LANES), f32),
        tap_out=vmem((n, chunk, LANES), bf16),
        tap_in=vmem((n, chunk, LANES), bf16),
        tap_all=vmem((n, chunk, LANES), bf16),
        dirs=vmem((m, rows, cols), bf16),
        ready=pltpu.SemaphoreType.REGULAR,
        x_s=dma((steps,)),
        f_s=dma((steps,)),
        v_in=dma((2,)),
        v_r=dma((lo - 1,)),
        pass_r=dma((lo - 1,)),
        turn_r=dma((lo - 1,)),
    )
    for name in ("g", "c", "w", "m", "k", "v", "pass", "turn"):
        scratch[name + "_s"] = dma
    for name in ("low", "halo", "near", "far", "gram", "tap", "all", "dir"):
        scratch[name + "_s"] = dma
        scratch[name + "_r"] = dma
    inputs = (x, v, g, c, f, w, m1, m2, k, k1, k2)
    inputs = [pltpu.with_memory_space_constraint(a, pltpu.HBM) for a in inputs]
    shape = jax.ShapeDtypeStruct
    between = (
        shape((rows, rank), bf16),
        shape((rank, rank), bf16),
        shape((rank, rank), bf16),
        shape(f.shape, bf16),
        shape(w.shape, f32),
        shape(m1.shape, f32),
        shape(m1.shape, f32),
        shape(k.shape, f32),
        shape(k.shape, f32),
        shape(k.shape, f32),
    )
    hbm = pl.BlockSpec(memory_space=pltpu.HBM)
    held = pl.BlockSpec(memory_space=pltpu.VMEM)
    results = pl.pallas_call(
        functools.partial(reduce_kernel, tuple(scratch), n, m, hi, lo),
        out_shape=between,
        in_specs=[hbm] * len(inputs),
        out_specs=(held,) * len(between),
        scratch_shapes=list(scratch.values()),
        compiler_params=pltpu.CompilerParams(
            collective_id=0, has_side_effects=True, vmem_limit_bytes=24 << 20
        ),
        name="reduce",
    )(*inputs)

    outputs = (
        shape(w.shape, f32),
        shape(w.shape, bf16),
        shape(w.shape, f32),
        shape(m1.shape, f32),
        shape(m1.shape, f32),
        shape(k.shape, f32),
        shape(k.shape, f32),
        shape(k.shape, f32),
    )
    return pl.pallas_call(
        functools.partial(update_kernel, steps, features * m),
        out_shape=outputs,
        in_specs=[held] * len(between),
        out_specs=(hbm,) * len(outputs),
        scratch_shapes=[
            vmem(w.shape, f32),
            vmem(w.shape, bf16),
            vmem(w.shape, f32),
            dma((5,)),
            dma((3,)),
        ],
        compiler_params=pltpu.CompilerParams(vmem_limit_bytes=24 << 20),
        name="update",
    )(*results)


def solution(mesh):
    both, rows, cols = P("fs", "tp"), P("fs", None), P(None, "tp")
    return jax.shard_map(
        functools.partial(body, mesh.shape["fs"], mesh.shape["tp"]),
        mesh=mesh,
        in_specs=(both, rows, both, both, P("tp", None), both, both, both, cols, cols, cols),
        out_specs=(both, both, both, both, both, cols, cols, cols),
        check_vma=False,
    )
```

time: 24.9 us -> 22.9 us (0.920)
  Pallas kernels: 24.1 us -> 22.1 us
    pallas_call x1, Pallas kernels: 21.9 us -> 20.1 us  [body(): pl.pallas_call(functools.partial(reduce_kernel, tuple(scratch), n, m, hi,...]
where the time goes in v2:
time: 22.9 us; the launch traced here: 22.8 us
  Pallas kernels  22.1 us (97%)
  between operations  0.65 us (3%)
    pallas_call x1, Pallas kernels, body(): pl.pallas_call(functools.partial(reduce_kernel, tuple(scratch), n, m, hi,...  20.1 us
    pallas_call x1, Pallas kernels, body(): pl.pallas_call(functools.partial(update_kernel, steps, features * m), out...  2.07 us

profile of v2, /device:TPU:0, one launch (start us, length us, event | category | flops | bytes accessed | tf_op | source)
XLA Modules:
  0.0 22.8 jit_solution(1675385360465570503)
XLA Ops:
  0.6 20.1 %reduce.1 = (bf16[128,256]{1,0:T(8,128)(2,1)S(1)}, bf16[256,256]{1,0:T(8,128)(2,1)S(1)}, bf16[256,256]{1,0:T(8,128)(2,1)S(1)}, bf16[2048,256]{1,0:T(8,128)(2,1)S...) custom-call(bf16[128,2048]{1,0:T(8,128)(2,1)} %refs_0_.1, ...), custom_call_target="tpu_custom_call" | custom-call | tf_op jit(solution)/shard_map/reduce/pallas_call | solution.py:480
  20.7 2.1 %update.1 = (f32[128,2048]{1,0:T(8,128)}, bf16[128,2048]{1,0:T(8,128)(2,1)}, f32[128,2048]{1,0:T(8,128)}, f32[128,128]{1,0:T(8,128)}, f32[128,128]{1,0:T(8,128)}...) custom-call(bf16[128,256]{1,0:T(8,128)(2,1)S(1)} %get-tuple-element.18.refs_0_, ...), custom_call_target="tpu_custom_call" | custom-call | tf_op jit(solution)/shard_map/update/pallas_call | solution.py:502

commit v3 on v2

--- a/solution.py
+++ b/solution.py
@@ -59,15 +59,14 @@
 
 def reduce_kernel(names, n, m, hi, lo, *refs):
     (x_hbm, v_hbm, g_hbm, c_hbm, f_hbm, w_hbm, m1_hbm, m2_hbm, k_hbm, k1_hbm, k2_hbm) = refs[:11]
-    (dir_ref, gh_ref, gl_ref, f_ref, w_ref, n1_ref, n2_ref, nk_ref, nk1_ref, nk2_ref) = refs[11:21]
-    s = types.SimpleNamespace(**dict(zip(names, refs[21:])))
+    (value_ref, copy_ref, step_ref, n1_ref, n2_ref, nk_ref, nk1_ref, nk2_ref) = refs[11:19]
+    s = types.SimpleNamespace(**dict(zip(names, refs[19:])))
     me = lax.axis_index("fs")
     my = lax.axis_index("tp")
     h, l = me // lo, lax.rem(me, lo)
     half = hi // 2
     near = h // half * half
     far = half - near
-    spot = me - near * lo
     tokens, features = s.x.shape
     rows, cols = s.m.shape[1:]
     reach = s.halo.shape[0]
@@ -85,6 +84,24 @@
     def lo_from(off):
         return lax.rem(l + lo - off, lo)
 
+    def mate(off):
+        return lax.rem(h - near + off, half)
+
+    def mate_from(off):
+        return lax.rem(h - near + half - off, half)
+
+    def tell(r):
+        @pl.when(h > 0)
+        def _():
+            pl.semaphore_signal(s.ready.at[r], inc=1, device_id={"fs": me - lo}, device_id_type=MESH)
+
+        @pl.when(h + 1 < hi)
+        def _():
+            pl.semaphore_signal(s.ready.at[r], inc=1, device_id={"fs": me + lo}, device_id_type=MESH)
+
+    def hear(r):
+        pl.semaphore_wait(s.ready.at[r], jnp.where(h > 0, 1, 0) + jnp.where(h + 1 < hi, 1, 0))
+
     def peers(count, own, fn):
         def step(off, carry):
             fn(off, lax.rem(own + off, count))
@@ -94,34 +111,9 @@
 
     spans = [pl.ds(i * block, block) for i in range(steps)]
     x_in = [copy(x_hbm.at[:, at], s.x.at[:, at], s.x_s.at[i]) for i, at in enumerate(spans)]
-    f_in = [copy(f_hbm.at[at], f_ref.at[at], s.f_s.at[i]) for i, at in enumerate(spans)]
-    for i in range(steps):
-        x_in[i].start()
-        f_in[i].start()
-
-    barrier = pltpu.get_barrier_semaphore()
-
-    def hello(axis, peer):
-        pl.semaphore_signal(barrier, inc=1, device_id={axis: peer}, device_id_type=MESH)
-
-    for off in range(1, hi):
-        hello("fs", lax.rem(h + off, hi) * lo + l)
-    for off in range(1, lo):
-        hello("fs", h * lo + lo_peer(off))
-
-    @pl.when(me + 1 < n)
-    def _():
-        hello("fs", me + 1)
-
-    @pl.when(me > 0)
-    def _():
-        hello("fs", me - 1)
-
-    for off in range(1, m):
-        hello("tp", lax.rem(my + off, m))
-
+    f_in = [copy(f_hbm.at[at], s.f.at[at], s.f_s.at[i]) for i, at in enumerate(spans)]
     width = half * lo * rows
-    near_at = pl.ds(pl.multiple_of(near * lo * rows, width), width)
+    plane = lo * rows
     far_at = pl.ds(pl.multiple_of(far * lo * rows, width), width)
     aligned = rows % LANES == 0
     if aligned:
@@ -137,16 +129,51 @@
         copy(v_hbm.at[:, far_at], s.v_all, s.v_in.at[0]).start()
     g_in = copy(g_hbm, s.g, s.g_s)
     c_in = copy(c_hbm, s.c, s.c_s)
-    v_in = copy(v_hbm.at[:, near_at], s.v_near, s.v_in.at[1])
     g_in.start()
+    for i in range(steps):
+        x_in[i].start()
+        f_in[i].start()
+
+    for i in range(half):
+        start = pl.multiple_of((near + i) * plane, plane)
+        copy(v_hbm.at[:, pl.ds(start, plane)], s.v_near.at[i], s.v_in.at[1]).start()
+
     c_in.start()
-    v_in.start()
+
+    barrier = pltpu.get_barrier_semaphore()
+
+    def hello(axis, peer):
+        pl.semaphore_signal(barrier, inc=1, device_id={axis: peer}, device_id_type=MESH)
+
+    for off in range(1, half):
+        hello("fs", (near + mate(off)) * lo + l)
+    for off in range(1, lo):
+        hello("fs", h * lo + lo_peer(off))
+
+    @pl.when(h == half - 1)
+    def _():
+        hello("fs", me + lo)
+
+    @pl.when(h == half)
+    def _():
+        hello("fs", me - lo)
+
+    @pl.when(me + 1 < n)
+    def _():
+        hello("fs", me + 1)
+
+    @pl.when(me > 0)
+    def _():
+        hello("fs", me - 1)
+
+    for off in range(1, m):
+        hello("tp", lax.rem(my + off, m))
 
     low = None
     for i, at in enumerate(spans):
         x_in[i].wait()
         f_in[i].wait()
-        product = jnp.dot(s.x[:, at], f_ref[at, :], preferred_element_type=f32)
+        product = jnp.dot(s.x[:, at], s.f[at, :], preferred_element_type=f32)
         low = product if low is None else low + product
     low = low.astype(bf16)
     for j in range(m):
@@ -159,10 +186,12 @@
             for p in range(lo):
                 at = (i * lo + p) * rows
                 s.v_far[p, :, i * rows : (i + 1) * rows] = s.v_all[:, at : at + rows]
+    landed(s.v_near, s.v_in.at[1])
     g_in.wait()
     c_in.wait()
 
-    greeted = (hi - 1) + (lo - 1) + (m - 1)
+    greeted = (half - 1) + (lo - 1) + (m - 1)
+    greeted = greeted + jnp.where(h == half - 1, 1, 0) + jnp.where(h == half, 1, 0)
     greeted = greeted + jnp.where(me + 1 < n, 1, 0) + jnp.where(me > 0, 1, 0)
     pl.semaphore_wait(barrier, greeted)
 
@@ -180,6 +209,20 @@
         halo_copy.start()
 
     share = pl.ds(my * piece, piece)
+
+    near_copies = [
+        remote(
+            s.v_near.at[mate(off), share],
+            s.v_mate.at[h - near, share],
+            s.mate_s,
+            s.mate_r.at[off - 1],
+            "fs",
+            (near + mate(off)) * lo + l,
+        )
+        for off in range(1, half)
+    ]
+    for one in near_copies:
+        one.start()
     v_copies = [
         remote(
             s.v_far.at[lo_peer(off), share],
@@ -194,15 +237,9 @@
     for one in v_copies:
         one.start()
 
-    for off in range(1, hi):
-        pl.semaphore_signal(
-            s.ready,
-            inc=1,
-            device_id={"fs": lax.rem(h + off, hi) * lo + l},
-            device_id_type=MESH,
-        )
-
-    w_in = copy(w_hbm, w_ref, s.w_s)
+    tell(0)
+
+    w_in = copy(w_hbm, s.w, s.w_s)
     w_in.start()
     for i, ref in enumerate((m1_hbm, m2_hbm)):
         copy(ref, s.m.at[i], s.m_s).start()
@@ -220,8 +257,12 @@
             right = s.cot[g, :count, :]
             sums = []
             for k in range(taps):
-                product = s.ext[g, pl.ds(reach - k, count), :] * right
-                sums.append(jnp.sum(product.reshape(count // SUBLANES, SUBLANES, LANES), axis=0))
+                used = min(-(-k // SUBLANES) * SUBLANES, count) if add else count
+                if used == 0:
+                    sums.append(jnp.zeros((SUBLANES, LANES), f32))
+                    continue
+                product = s.ext[g, pl.ds(reach - k, used), :] * right[:used]
+                sums.append(jnp.sum(product.reshape(used // SUBLANES, SUBLANES, LANES), axis=0))
             sums += [jnp.zeros((SUBLANES, LANES), f32)] * (padded - taps)
             at = pl.ds(pl.multiple_of(g * padded, padded), padded)
             total = column_sums(sums)
@@ -252,13 +293,40 @@
     ]
     for one in turn_copies:
         one.start()
+    s.level[h - near] = turned
+    level_copies = [
+        remote(
+            s.level.at[h - near],
+            s.level.at[h - near],
+            s.level_s,
+            s.level_r.at[off - 1],
+            "fs",
+            (near + mate(off)) * lo + l,
+        )
+        for off in range(1, half)
+    ]
+    for one in level_copies:
+        one.start()
+
+    hear(0)
+    tell(1)
 
     lax.fori_loop(early, groups, group_step(tokens, False), 0)
 
-    v_in.wait()
-    direct = jnp.dot(turned, s.v_near[...], preferred_element_type=f32)
-    for j in range(half * lo):
-        s.near_out[j] = direct[:, j * rows : (j + 1) * rows].astype(bf16)
+    for r in range(1, hi - 2):
+        hear(r)
+        tell(r + 1)
+
+    s.gram[my] = lax.dot_general(s.f[...], s.f[...], FIRST, preferred_element_type=f32)
+    for off in range(1, m):
+        remote(s.gram.at[my], s.gram.at[my], s.gram_s, s.gram_r, "tp", lax.rem(my + off, m)).start()
+
+
+    for off in range(1, half):
+        near_copies[off - 1].wait_recv()
+        at = s.v_mate.at[mate_from(off), share]
+        for t in range(1, m):
+            remote(at, at, s.lift_s, s.lift_r.at[off - 1], "tp", lax.rem(my + t, m)).start()
 
     @pl.when(me > 0)
     def _():
@@ -275,19 +343,13 @@
     lax.fori_loop(0, groups, group_step(reach, True), 0)
     s.tap_out[...] = s.stage[...].reshape(s.tap_out.shape).astype(bf16)
 
-    pl.semaphore_wait(s.ready, hi - 1)
+    hear(hi - 2)
 
     def send_taps(off, p):
         remote(s.tap_out.at[p], s.tap_in.at[me], s.tap_s, s.tap_r, "fs", p).start()
 
     peers(n, me, send_taps)
     s.tap_in[me] = s.tap_out[me]
-
-    def send_near(off, p):
-        remote(s.near_out.at[p], s.near_in.at[spot], s.near_s, s.near_r, "fs", near * lo + p).start()
-
-    peers(half * lo, spot, send_near)
-    s.near_in[spot] = s.near_out[spot]
 
     for off in range(1, lo):
         v_copies[off - 1].wait_recv()
@@ -308,9 +370,25 @@
             s.far_out.at[i], s.far_in.at[h - near], s.far_s, s.far_r, "fs", (far + i) * lo + l
         ).start()
 
-    s.gram[my] = lax.dot_general(f_ref[...], f_ref[...], FIRST, preferred_element_type=f32)
-    for off in range(1, m):
-        remote(s.gram.at[my], s.gram.at[my], s.gram_s, s.gram_r, "tp", lax.rem(my + off, m)).start()
+    direct = jnp.dot(turned, s.v_near[h - near], preferred_element_type=f32)
+    for off in range(1, half):
+        i = mate_from(off)
+        landed(s.v_mate.at[i, pl.ds(0, tokens - piece)], s.lift_r.at[off - 1])
+        level_copies[off - 1].wait_recv()
+        direct = direct + jnp.dot(s.level[i], s.v_mate[i], preferred_element_type=f32)
+    for p in range(lo):
+        s.near_out[p] = direct[:, p * rows : (p + 1) * rows].astype(bf16)
+
+    for off in range(1, lo):
+        remote(
+            s.near_out.at[lo_peer(off)],
+            s.near_in.at[l],
+            s.near_s,
+            s.near_r,
+            "fs",
+            h * lo + lo_peer(off),
+        ).start()
+    s.near_in[l] = s.near_out[l]
 
     landed(s.tap_in.at[pl.ds(0, n - 1)], s.tap_r)
     s.tap_all[me] = jnp.sum(s.tap_in[...].astype(f32), axis=0).astype(bf16)
@@ -325,15 +403,15 @@
     for j in range(1, m):
         total = total + s.gram[j]
     top = total.astype(bf16)
-    gh_ref[...] = top
-    gl_ref[...] = (total - top.astype(f32)).astype(bf16)
+    s.top[...] = top
+    s.rest[...] = (total - top.astype(f32)).astype(bf16)
     w_in.wait()
     landed(s.m, s.m_s)
     landed(s.k, s.k_s)
 
-    landed(s.near_in.at[pl.ds(0, half * lo - 1)], s.near_r)
+    landed(s.near_in.at[pl.ds(0, lo - 1)], s.near_r)
     projected = s.near_in[0].astype(f32)
-    for j in range(1, half * lo):
+    for j in range(1, lo):
         projected = projected + s.near_in[j].astype(f32)
     landed(s.far_in, s.far_r)
     for i in range(half):
@@ -347,6 +425,20 @@
     n1_ref[...] = first
     n2_ref[...] = second
 
+    landed(s.dirs.at[pl.ds(0, m - 1)], s.dir_s)
+    landed(s.dirs.at[pl.ds(0, m - 1)], s.dir_r)
+    direction = jnp.concatenate([s.dirs[j] for j in range(m)], axis=1)
+    moved = jnp.dot(direction, s.top[...], preferred_element_type=f32)
+    moved = moved + jnp.dot(direction, s.rest[...], preferred_element_type=f32)
+    mean = jnp.sum(moved * direction.astype(f32), axis=1, keepdims=True) / (features * m)
+    scale = lax.rsqrt(mean + 0.01)
+    for at in spans:
+        step = lax.dot_general(direction, s.f[at, :], LAST, preferred_element_type=f32) * scale
+        step_ref[:, at] = step
+        value = s.w[:, at] - 0.05 * step
+        value_ref[:, at] = value
+        copy_ref[:, at] = value.astype(bf16)
+
     @pl.when(me + 1 < n)
     def _():
         halo_copy.wait_send()
@@ -355,7 +447,10 @@
     landed(s.v_far.at[pl.ds(0, lo - 1), share], s.v_s)
     landed(s.v_far.at[pl.ds(0, lo - 1), pl.ds(0, tokens - piece)], s.pass_s)
     landed(s.turned.at[pl.ds(0, lo - 1)], s.turn_s)
-    landed(s.near_out.at[pl.ds(0, half * lo - 1)], s.near_s)
+    landed(s.near_out.at[pl.ds(0, lo - 1)], s.near_s)
+    landed(s.v_near.at[pl.ds(0, half - 1), share], s.mate_s)
+    landed(s.v_near.at[pl.ds(0, half - 1), pl.ds(0, tokens - piece)], s.lift_s)
+    landed(s.level.at[pl.ds(0, half - 1)], s.level_s)
     landed(s.far_out, s.far_s)
     landed(s.gram.at[pl.ds(0, m - 1)], s.gram_s)
     landed(s.tap_out.at[pl.ds(0, n - 1)], s.tap_s)
@@ -372,39 +467,14 @@
         nk2_ref[:, lanes] = second
         nk_ref[:, lanes] = s.k[0, :, lanes] - 0.05 * first * lax.rsqrt(second)
 
-    landed(s.dirs.at[pl.ds(0, m - 1)], s.dir_s)
-    landed(s.dirs.at[pl.ds(0, m - 1)], s.dir_r)
-    for j in range(m):
-        dir_ref[:, j * cols : (j + 1) * cols] = s.dirs[j]
-
-
-def update_kernel(steps, width, *refs):
-    dir_ref, gh_ref, gl_ref, f_ref, w_ref = refs[:5]
-    small, target, made = refs[5:10], refs[10:18], refs[18:21]
-    small_s, wide_s = refs[21:]
-    value_ref, copy_ref, step_ref = made
-    copy = pltpu.make_async_copy
-    for j in range(5):
-        copy(small[j], target[3 + j], small_s.at[j]).start()
-    direction = dir_ref[...]
-    turned = jnp.dot(direction, gh_ref[...], preferred_element_type=f32)
-    turned = turned + jnp.dot(direction, gl_ref[...], preferred_element_type=f32)
-    mean = jnp.sum(turned * direction.astype(f32), axis=1, keepdims=True) / width
-    scale = lax.rsqrt(mean + 0.01)
-    block = f_ref.shape[0] // steps
-    for i in range(steps):
-        at = pl.ds(i * block, block)
-        step = lax.dot_general(direction, f_ref[at, :], LAST, preferred_element_type=f32) * scale
-        step_ref[:, at] = step
-        value = w_ref[:, at] - 0.05 * step
-        value_ref[:, at] = value
-        copy_ref[:, at] = value.astype(bf16)
-        for j in range(3):
-            copy(made[j].at[:, at], target[j].at[:, at], wide_s.at[j]).start()
-    for j in range(5):
-        copy(small[j], target[3 + j], small_s.at[j]).wait()
-    for j in range(3):
-        copy(made[j], target[j], wide_s.at[j]).wait()
+
+def store_kernel(*refs):
+    source, target, sems = refs[:8], refs[8:16], refs[16]
+    outs = [pltpu.make_async_copy(source[j], target[j], sems.at[j]) for j in range(8)]
+    for out in outs:
+        out.start()
+    for out in outs:
+        out.wait()
 
 
 def body(n, m, x, v, g, c, f, w, m1, m2, k, k1, k2):
@@ -423,8 +493,14 @@
     width = half * lo * rows
     scratch = dict(
         x=vmem(x.shape, x.dtype),
+        f=vmem(f.shape, f.dtype),
+        w=vmem(w.shape, f32),
+        top=vmem((rank, rank), bf16),
+        rest=vmem((rank, rank), bf16),
         v_all=vmem((tokens, width) if rows % LANES else (16, LANES), bf16),
-        v_near=vmem((tokens, width), bf16),
+        v_near=vmem((half, tokens, lo * rows), bf16),
+        v_mate=vmem((half, tokens, lo * rows), bf16),
+        level=vmem((half, cols, tokens), bf16),
         v_far=vmem((lo, tokens, half * rows), bf16),
         v_got=vmem((lo, tokens, half * rows), bf16),
         g=vmem(g.shape, g.dtype),
@@ -435,8 +511,8 @@
         low_in=vmem((m, tokens, cols), bf16),
         turned=vmem((lo, cols, tokens), bf16),
         gram=vmem((m, rank, rank), f32),
-        near_out=vmem((half * lo, cols, rows), bf16),
-        near_in=vmem((half * lo, cols, rows), bf16),
+        near_out=vmem((lo, cols, rows), bf16),
+        near_in=vmem((lo, cols, rows), bf16),
         far_out=vmem((half, cols, rows), bf16),
         far_in=vmem((half, cols, rows), bf16),
         halo=vmem((reach, channels), bf16),
@@ -447,15 +523,18 @@
         tap_in=vmem((n, chunk, LANES), bf16),
         tap_all=vmem((n, chunk, LANES), bf16),
         dirs=vmem((m, rows, cols), bf16),
-        ready=pltpu.SemaphoreType.REGULAR,
+        ready=pltpu.SemaphoreType.REGULAR((hi - 1,)),
         x_s=dma((steps,)),
         f_s=dma((steps,)),
         v_in=dma((2,)),
         v_r=dma((lo - 1,)),
         pass_r=dma((lo - 1,)),
         turn_r=dma((lo - 1,)),
+        mate_r=dma((half - 1,)),
+        lift_r=dma((half - 1,)),
+        level_r=dma((half - 1,)),
     )
-    for name in ("g", "c", "w", "m", "k", "v", "pass", "turn"):
+    for name in ("g", "c", "w", "m", "k", "v", "pass", "turn", "mate", "lift", "level"):
         scratch[name + "_s"] = dma
     for name in ("low", "halo", "near", "far", "gram", "tap", "all", "dir"):
         scratch[name + "_s"] = dma
@@ -464,10 +543,8 @@
     inputs = [pltpu.with_memory_space_constraint(a, pltpu.HBM) for a in inputs]
     shape = jax.ShapeDtypeStruct
     between = (
-        shape((rows, rank), bf16),
-        shape((rank, rank), bf16),
-        shape((rank, rank), bf16),
-        shape(f.shape, bf16),
+        shape(w.shape, f32),
+        shape(w.shape, bf16),
         shape(w.shape, f32),
         shape(m1.shape, f32),
         shape(m1.shape, f32),
@@ -489,30 +566,14 @@
         name="reduce",
     )(*inputs)
 
-    outputs = (
-        shape(w.shape, f32),
-        shape(w.shape, bf16),
-        shape(w.shape, f32),
-        shape(m1.shape, f32),
-        shape(m1.shape, f32),
-        shape(k.shape, f32),
-        shape(k.shape, f32),
-        shape(k.shape, f32),
-    )
     return pl.pallas_call(
-        functools.partial(update_kernel, steps, features * m),
-        out_shape=outputs,
+        store_kernel,
+        out_shape=between,
         in_specs=[held] * len(between),
-        out_specs=(hbm,) * len(outputs),
-        scratch_shapes=[
-            vmem(w.shape, f32),
-            vmem(w.shape, bf16),
-            vmem(w.shape, f32),
-            dma((5,)),
-            dma((3,)),
-        ],
-        compiler_params=pltpu.CompilerParams(vmem_limit_bytes=24 << 20),
-        name="update",
+        out_specs=(hbm,) * len(between),
+        scratch_shapes=[dma((len(between),))],
+        compiler_params=pltpu.CompilerParams(vmem_limit_bytes=16 << 20),
+        name="store",
     )(*results)
 
 

time: 22.9 us -> 22.1 us (0.965)
  Pallas kernels: 22.1 us -> 21.3 us
    pallas_call x1, Pallas kernels: 20.1 us -> 19.5 us  [body(): pl.pallas_call(functools.partial(reduce_kernel, tuple(scratch), n, m, hi,...]
    pallas_call x1, Pallas kernels: 2.07 us -> 1.72 us  [body(): pl.pallas_call(store_kernel, out_shape=between, in_specs=[held] * len(bet...]
where the time goes in v3:
time: 22.1 us; the launch traced here: 21.9 us
  Pallas kernels  21.3 us (96%)
  between operations  0.65 us (3%)
    pallas_call x1, Pallas kernels, body(): pl.pallas_call(functools.partial(reduce_kernel, tuple(scratch), n, m, hi,...  19.5 us
    pallas_call x1, Pallas kernels, body(): pl.pallas_call(store_kernel, out_shape=between, in_specs=[held] * len(bet...  1.72 us

profile of v3, /device:TPU:0, one launch (start us, length us, event | category | flops | bytes accessed | tf_op | source)
XLA Modules:
  0.0 21.9 jit_solution(1564839111448104489)
XLA Ops:
  0.6 19.5 %reduce.1 = (f32[128,2048]{1,0:T(8,128)S(1)}, bf16[128,2048]{1,0:T(8,128)(2,1)S(1)}, f32[128,2048]{1,0:T(8,128)S(1)}, f32[128,128]{1,0:T(8,128)S(1)}, f32[128,12...) custom-call(bf16[128,2048]{1,0:T(8,128)(2,1)} %refs_0_.1, ...), custom_call_target="tpu_custom_call" | custom-call | tf_op jit(solution)/shard_map/reduce/pallas_call | solution.py:557
  20.2 1.7 %store.1 = (f32[128,2048]{1,0:T(8,128)}, bf16[128,2048]{1,0:T(8,128)(2,1)}, f32[128,2048]{1,0:T(8,128)}, f32[128,128]{1,0:T(8,128)}, f32[128,128]{1,0:T(8,128)},...) custom-call(f32[128,2048]{1,0:T(8,128)S(1)} %get-tuple-element.16.refs_0_, ...), custom_call_target="tpu_custom_call" | custom-call | tf_op jit(solution)/shard_map/store/pallas_call | solution.py:569

commit v4 on v3

--- a/solution.py
+++ b/solution.py
@@ -68,6 +68,7 @@
     near = h // half * half
     far = half - near
     tokens, features = s.x.shape
+    rank = s.f.shape[1]
     rows, cols = s.m.shape[1:]
     reach = s.halo.shape[0]
     groups = s.ext.shape[0]
@@ -110,7 +111,7 @@
         lax.fori_loop(1, count, step, 0)
 
     spans = [pl.ds(i * block, block) for i in range(steps)]
-    x_in = [copy(x_hbm.at[:, at], s.x.at[:, at], s.x_s.at[i]) for i, at in enumerate(spans)]
+    x_in = [copy(x_hbm.at[:, at], s.x.at[:, at], s.f_s.at[i]) for i, at in enumerate(spans)]
     f_in = [copy(f_hbm.at[at], s.f.at[at], s.f_s.at[i]) for i, at in enumerate(spans)]
     width = half * lo * rows
     plane = lo * rows
@@ -169,15 +170,15 @@
     for off in range(1, m):
         hello("tp", lax.rem(my + off, m))
 
-    low = None
-    for i, at in enumerate(spans):
-        x_in[i].wait()
-        f_in[i].wait()
-        product = jnp.dot(s.x[:, at], s.f[at, :], preferred_element_type=f32)
-        low = product if low is None else low + product
-    low = low.astype(bf16)
-    for j in range(m):
-        s.low_out[j] = low[:, j * cols : (j + 1) * cols]
+    def multiply(low, first, last):
+        for i in range(first, last):
+            landed(s.f.at[pl.ds(0, block + tokens * block // rank)], s.f_s.at[i])
+            at = spans[i]
+            product = jnp.dot(s.x[:, at], s.f[at, :], preferred_element_type=f32)
+            low = product if low is None else low + product
+        return low
+
+    low = multiply(None, 0, steps // 2)
     if aligned:
         landed(s.v_far, s.v_in.at[0])
     else:
@@ -186,30 +187,49 @@
             for p in range(lo):
                 at = (i * lo + p) * rows
                 s.v_far[p, :, i * rows : (i + 1) * rows] = s.v_all[:, at : at + rows]
-    landed(s.v_near, s.v_in.at[1])
     g_in.wait()
-    c_in.wait()
 
     greeted = (half - 1) + (lo - 1) + (m - 1)
     greeted = greeted + jnp.where(h == half - 1, 1, 0) + jnp.where(h == half, 1, 0)
     greeted = greeted + jnp.where(me + 1 < n, 1, 0) + jnp.where(me > 0, 1, 0)
     pl.semaphore_wait(barrier, greeted)
 
+    halo_copy = remote(
+        s.g.at[pl.ds(tokens - reach, reach)], s.halo, s.halo_s, s.halo_r, "fs", lax.rem(me + 1, n)
+    )
+
+    @pl.when(me + 1 < n)
+    def _():
+        halo_copy.start()
+
+    share = pl.ds(my * piece, piece)
+
+    v_copies = [
+        remote(
+            s.v_far.at[lo_peer(off), share],
+            s.v_got.at[l, share],
+            s.v_s,
+            s.v_r.at[off - 1],
+            "fs",
+            h * lo + lo_peer(off),
+        )
+        for off in range(1, lo)
+    ]
+    for one in v_copies[::-1]:
+        one.start()
+
+    tell(0)
+
+    low = multiply(low, steps // 2, steps)
+    low = low.astype(bf16)
+    for j in range(m):
+        s.low_out[j] = low[:, j * cols : (j + 1) * cols]
     for off in range(1, m):
         p = lax.rem(my + off, m)
         remote(s.low_out.at[p], s.low_in.at[my], s.low_s, s.low_r, "tp", p).start()
     s.low_in[my] = s.low_out[my]
 
-    halo_copy = remote(
-        s.g.at[pl.ds(tokens - reach, reach)], s.halo, s.halo_s, s.halo_r, "fs", lax.rem(me + 1, n)
-    )
-
-    @pl.when(me + 1 < n)
-    def _():
-        halo_copy.start()
-
-    share = pl.ds(my * piece, piece)
-
+    landed(s.v_near, s.v_in.at[1])
     near_copies = [
         remote(
             s.v_near.at[mate(off), share],
@@ -223,22 +243,7 @@
     ]
     for one in near_copies:
         one.start()
-    v_copies = [
-        remote(
-            s.v_far.at[lo_peer(off), share],
-            s.v_got.at[l, share],
-            s.v_s,
-            s.v_r.at[off - 1],
-            "fs",
-            h * lo + lo_peer(off),
-        )
-        for off in range(1, lo)
-    ]
-    for one in v_copies:
-        one.start()
-
-    tell(0)
-
+    c_in.wait()
     w_in = copy(w_hbm, s.w, s.w_s)
     w_in.start()
     for i, ref in enumerate((m1_hbm, m2_hbm)):
@@ -298,7 +303,7 @@
         remote(
             s.level.at[h - near],
             s.level.at[h - near],
-            s.level_s,
+            s.turn_s,
             s.level_r.at[off - 1],
             "fs",
             (near + mate(off)) * lo + l,
@@ -326,7 +331,7 @@
         near_copies[off - 1].wait_recv()
         at = s.v_mate.at[mate_from(off), share]
         for t in range(1, m):
-            remote(at, at, s.lift_s, s.lift_r.at[off - 1], "tp", lax.rem(my + t, m)).start()
+            remote(at, at, s.mate_s, s.lift_r.at[off - 1], "tp", lax.rem(my + t, m)).start()
 
     @pl.when(me > 0)
     def _():
@@ -355,7 +360,7 @@
         v_copies[off - 1].wait_recv()
         at = s.v_got.at[lo_from(off), share]
         for t in range(1, m):
-            remote(at, at, s.pass_s, s.pass_r.at[off - 1], "tp", lax.rem(my + t, m)).start()
+            remote(at, at, s.v_s, s.pass_r.at[off - 1], "tp", lax.rem(my + t, m)).start()
 
     acc = jnp.dot(s.turned[l], s.v_far[l], preferred_element_type=f32)
     for off in range(1, lo):
@@ -444,13 +449,10 @@
         halo_copy.wait_send()
 
     landed(s.low_out.at[pl.ds(0, m - 1)], s.low_s)
-    landed(s.v_far.at[pl.ds(0, lo - 1), share], s.v_s)
-    landed(s.v_far.at[pl.ds(0, lo - 1), pl.ds(0, tokens - piece)], s.pass_s)
-    landed(s.turned.at[pl.ds(0, lo - 1)], s.turn_s)
+    landed(s.v_far.at[pl.ds(0, lo - 1)], s.v_s)
+    landed(s.sent.at[pl.ds(0, lo + half - 2)], s.turn_s)
     landed(s.near_out.at[pl.ds(0, lo - 1)], s.near_s)
-    landed(s.v_near.at[pl.ds(0, half - 1), share], s.mate_s)
-    landed(s.v_near.at[pl.ds(0, half - 1), pl.ds(0, tokens - piece)], s.lift_s)
-    landed(s.level.at[pl.ds(0, half - 1)], s.level_s)
+    landed(s.v_near.at[pl.ds(0, half - 1)], s.mate_s)
     landed(s.far_out, s.far_s)
     landed(s.gram.at[pl.ds(0, m - 1)], s.gram_s)
     landed(s.tap_out.at[pl.ds(0, n - 1)], s.tap_s)
@@ -501,6 +503,7 @@
         v_near=vmem((half, tokens, lo * rows), bf16),
         v_mate=vmem((half, tokens, lo * rows), bf16),
         level=vmem((half, cols, tokens), bf16),
+        sent=vmem((lo + half, cols, tokens), bf16),
         v_far=vmem((lo, tokens, half * rows), bf16),
         v_got=vmem((lo, tokens, half * rows), bf16),
         g=vmem(g.shape, g.dtype),
@@ -524,7 +527,6 @@
         tap_all=vmem((n, chunk, LANES), bf16),
         dirs=vmem((m, rows, cols), bf16),
         ready=pltpu.SemaphoreType.REGULAR((hi - 1,)),
-        x_s=dma((steps,)),
         f_s=dma((steps,)),
         v_in=dma((2,)),
         v_r=dma((lo - 1,)),
@@ -534,7 +536,7 @@
         lift_r=dma((half - 1,)),
         level_r=dma((half - 1,)),
     )
-    for name in ("g", "c", "w", "m", "k", "v", "pass", "turn", "mate", "lift", "level"):
+    for name in ("g", "c", "w", "m", "k", "v", "turn", "mate"):
         scratch[name + "_s"] = dma
     for name in ("low", "halo", "near", "far", "gram", "tap", "all", "dir"):
         scratch[name + "_s"] = dma

time: 22.1 us -> 21.9 us (level)
  no operation moved by 1% of the time
where the time goes in v4:
time: 21.9 us; the launch traced here: 21.8 us
  Pallas kernels  21.1 us (96%)
  between operations  0.65 us (3%)
    pallas_call x1, Pallas kernels, body(): pl.pallas_call(functools.partial(reduce_kernel, tuple(scratch), n, m, hi,...  19.4 us
    pallas_call x1, Pallas kernels, body(): pl.pallas_call(store_kernel, out_shape=between, in_specs=[held] * len(bet...  1.72 us

profile of v4, /device:TPU:0, one launch (start us, length us, event | category | flops | bytes accessed | tf_op | source)
XLA Modules:
  0.0 21.8 jit_solution(16758941560872902023)
XLA Ops:
  0.6 19.4 %reduce.1 = (f32[128,2048]{1,0:T(8,128)S(1)}, bf16[128,2048]{1,0:T(8,128)(2,1)S(1)}, f32[128,2048]{1,0:T(8,128)S(1)}, f32[128,128]{1,0:T(8,128)S(1)}, f32[128,12...) custom-call(bf16[128,2048]{1,0:T(8,128)(2,1)} %refs_0_.1, ...), custom_call_target="tpu_custom_call" | custom-call | tf_op jit(solution)/shard_map/reduce/pallas_call | solution.py:559
  20.1 1.7 %store.1 = (f32[128,2048]{1,0:T(8,128)}, bf16[128,2048]{1,0:T(8,128)(2,1)}, f32[128,2048]{1,0:T(8,128)}, f32[128,128]{1,0:T(8,128)}, f32[128,128]{1,0:T(8,128)},...) custom-call(f32[128,2048]{1,0:T(8,128)S(1)} %get-tuple-element.16.refs_0_, ...), custom_call_target="tpu_custom_call" | custom-call | tf_op jit(solution)/shard_map/store/pallas_call | solution.py:571

commit v5 on v4

--- a/solution.py
+++ b/solution.py
@@ -215,8 +215,8 @@
         )
         for off in range(1, lo)
     ]
-    for one in v_copies[::-1]:
-        one.start()
+    for off in (2, 1, 3) if lo == 4 else range(1, lo):
+        v_copies[off - 1].start()
 
     tell(0)
 

time: 21.9 us -> 21.9 us (level)
  no operation moved by 1% of the time
where the time goes in v5:
time: 21.9 us; the launch traced here: 21.8 us
  Pallas kernels  21.1 us (96%)
  between operations  0.65 us (3%)
    pallas_call x1, Pallas kernels, body(): pl.pallas_call(functools.partial(reduce_kernel, tuple(scratch), n, m, hi,...  19.4 us
    pallas_call x1, Pallas kernels, body(): pl.pallas_call(store_kernel, out_shape=between, in_specs=[held] * len(bet...  1.72 us

profile of v5, /device:TPU:0, one launch (start us, length us, event | category | flops | bytes accessed | tf_op | source)
XLA Modules:
  0.0 21.8 jit_solution(6199718300297068550)
XLA Ops:
  0.6 19.4 %reduce.1 = (f32[128,2048]{1,0:T(8,128)S(1)}, bf16[128,2048]{1,0:T(8,128)(2,1)S(1)}, f32[128,2048]{1,0:T(8,128)S(1)}, f32[128,128]{1,0:T(8,128)S(1)}, f32[128,12...) custom-call(bf16[128,2048]{1,0:T(8,128)(2,1)} %refs_0_.1, ...), custom_call_target="tpu_custom_call" | custom-call | tf_op jit(solution)/shard_map/reduce/pallas_call | solution.py:559
  20.1 1.7 %store.1 = (f32[128,2048]{1,0:T(8,128)}, bf16[128,2048]{1,0:T(8,128)(2,1)}, f32[128,2048]{1,0:T(8,128)}, f32[128,128]{1,0:T(8,128)}, f32[128,128]{1,0:T(8,128)},...) custom-call(f32[128,2048]{1,0:T(8,128)S(1)} %get-tuple-element.16.refs_0_, ...), custom_call_target="tpu_custom_call" | custom-call | tf_op jit(solution)/shard_map/store/pallas_call | solution.py:571
